TPU v7x, 32 devices: a whole 2x2x4 slice. The times are simulated.
32 devices in a mesh: grp: 2 (over y), sp: 4 (over z), dp: 4 (over x, core).
Axes of the slice: x: 2, y: 2, z: 4, core: 2. Of those that a mesh axis runs over, the one named last changes fastest.
Arguments:
- tokens: bfloat16 [8, 640, 2048], P(('grp', 'dp'), 'sp'), parts along dimension 0, may hold values from -6 to 6
- query_weight: bfloat16 [2048, 1024], P('dp'), may hold values from -0.125 to 0.125
- key_weight: bfloat16 [2048, 256], P('dp'), may hold values from -0.125 to 0.125
- value_weight: bfloat16 [2048, 256], P('dp'), may hold values from -0.125 to 0.125
- out_weight: bfloat16 [1024, 2048], P(None, 'dp'), may hold values from -0.1875 to 0.1875
- query_gain: float32 [64], replicated, may hold values from 0.28 to 6
- key_gain: float32 [64], replicated, may hold values from 0.28 to 6
Outputs:
- mixed: bfloat16 [8, 640, 2048], P(('grp', 'dp'), 'sp'), parts along dimension 0
There are 2 independent parts, one for each index of `grp`. A program takes and returns all parts, laid end to end along the dimension named above; an argument that names none is the same for every part. Nothing has to cross between parts.
All inputs are finite; a program needn't handle non-finite values.
Results may differ from a plain program's by a relative error of at most 0.006.
The roundings to bfloat16 on the way count: a program that leaves them out, or rounds other values in their place, can miss the bound.
Values may be sent and summed in bfloat16 or wider, within the bound.
A program may use at most 64 MiB of HBM per device.

v0:
```python
import jax
import jax.numpy as jnp
from jax import lax
from jax.sharding import PartitionSpec as P

HEADS = 16
KV_HEADS = 4
HEAD_DIM = 64
GRID_W = 64


theta_base = 10000.0
norm_eps = 1e-06


def rotary_tables(positions):
    quarter = HEAD_DIM // 4
    inverse = theta_base ** (-jnp.arange(quarter, dtype=jnp.float32) / quarter)
    grid_rows = (positions // GRID_W).astype(jnp.float32)
    grid_cols = (positions % GRID_W).astype(jnp.float32)
    angles = jnp.concatenate([grid_rows[:, None] * inverse, grid_cols[:, None] * inverse], axis=-1)
    return (jnp.cos(angles), jnp.sin(angles))


def norm_rotate(raw, gain, cosine, sine):
    scaled = raw * lax.rsqrt(jnp.mean(raw * raw, axis=-1, keepdims=True) + norm_eps) * gain
    half = HEAD_DIM // 2
    first_half = scaled[..., :half]
    second_half = scaled[..., half:]
    cosine = cosine[:, None, :]
    sine = sine[:, None, :]
    turned = jnp.concatenate(
        [first_half * cosine - second_half * sine, second_half * cosine + first_half * sine],
        axis=-1,
    )
    return turned.astype(jnp.bfloat16)


def attend_block(queries, keys, values):
    scale = HEAD_DIM ** (-0.5)
    scores = jnp.einsum("qkgd,skd->kgqs", queries, keys, preferred_element_type=jnp.float32) * scale
    top = jnp.max(scores, axis=-1, keepdims=True)
    weights = jnp.exp(scores - top)
    probs = (weights / jnp.sum(weights, axis=-1, keepdims=True)).astype(jnp.bfloat16)
    result = jnp.einsum("kgqs,skd->qkgd", probs, values, preferred_element_type=jnp.float32).astype(
        jnp.bfloat16
    )
    return result.reshape(queries.shape[0], -1)


def shards(tokens, query_weight, key_weight, value_weight, out_weight, query_gain, key_gain):
    tok_rows = tokens.shape[1]
    local_rows = tokens.reshape(tok_rows, tokens.shape[2])
    seq_index = lax.axis_index("sp")
    per_kv = HEADS // KV_HEADS
    pieces = (
        lax.all_gather(query_weight, "dp", axis=0, tiled=True),
        lax.all_gather(key_weight, "dp", axis=0, tiled=True),
        lax.all_gather(value_weight, "dp", axis=0, tiled=True),
    )
    raw_q, raw_k, raw_v = tuple(
        (jnp.dot(local_rows, piece, preferred_element_type=jnp.float32) for piece in pieces)
    )
    positions = seq_index * tok_rows + jnp.arange(tok_rows, dtype=jnp.int32)
    cosine, sine = rotary_tables(positions)
    queries = norm_rotate(raw_q.reshape(tok_rows, HEADS, HEAD_DIM), query_gain, cosine, sine)
    keys = norm_rotate(raw_k.reshape(tok_rows, KV_HEADS, HEAD_DIM), key_gain, cosine, sine)
    values = raw_v.astype(jnp.bfloat16).reshape(tok_rows, KV_HEADS, HEAD_DIM)
    kv_pair = jnp.stack(
        [
            keys.reshape(tok_rows, KV_HEADS * HEAD_DIM),
            values.reshape(tok_rows, KV_HEADS * HEAD_DIM),
        ],
        axis=1,
    )
    whole_kv = lax.all_gather(kv_pair, "sp", axis=0, tiled=True)
    length = whole_kv.shape[0]
    all_k = whole_kv[:, 0].reshape(length, KV_HEADS, HEAD_DIM).transpose(1, 0, 2)[:, :, None, :]
    all_v = whole_kv[:, 1].reshape(length, KV_HEADS, HEAD_DIM).transpose(1, 0, 2)[:, :, None, :]
    grouped_q = queries.reshape(tok_rows, KV_HEADS, 1, per_kv, HEAD_DIM).transpose(1, 0, 2, 3, 4)

    def kv_head(operands):
        block_q, block_k, block_v = operands
        return attend_block(block_q, block_k, block_v)

    per_head = lax.map(kv_head, (grouped_q, all_k, all_v))
    attended = per_head.transpose(1, 0, 2).reshape(tok_rows, HEADS * HEAD_DIM)
    result = jnp.dot(
        attended,
        lax.all_gather(out_weight, "dp", axis=1, tiled=True),
        preferred_element_type=jnp.float32,
    )
    return result.astype(jnp.bfloat16).reshape(1, tok_rows, result.shape[1])


def solution(mesh):
    in_specs = (
        P(("grp", "dp"), "sp", None),
        P("dp", None),
        P("dp", None),
        P("dp", None),
        P(None, "dp"),
        P(),
        P(),
    )
    out_specs = P(("grp", "dp"), "sp", None)
    return jax.shard_map(shards, mesh=mesh, in_specs=in_specs, out_specs=out_specs, check_vma=False)
```

profile of v0, /device:TPU:0, one launch (start us, length us, event | category | flops | bytes accessed | tf_op | source)
XLA Modules:
  0.0 129.0 jit_solution(7905603839353737578)
XLA Ops:
  6.5 0.0 copy-start
  6.5 0.0 all-gather.5.cloned.1.call-start
  6.5 0.7 all-gather.5.cloned.1.call-update
  7.3 0.0 all-gather.7.cloned.1.call-start
  7.3 0.7 all-gather.7.cloned.1.call-update
  8.0 0.0 all-gather.9.cloned.1.call-start
  8.1 0.7 all-gather.9.cloned.1.call-update
  8.7 0.0 all-gather.11.cloned.1.call-start
  8.8 0.5 all-gather.11.cloned.1.call-update
  9.4 0.1 broadcast_multiply_fusion.1
  9.4 0.1 fusion.22
  9.6 18.8 %all-gather.5.cloned.1.call-done = bf16[2048,256]{1,0:T(8,128)(2,1)} async-done(((bf16[512,256]{1,0:T(8,128)(2,1)}), bf16[2048,256]{1,0:T(8,128)(2,1)}) %all-gather.5.cloned.1.call-update) | async-done | bytes 1048592 | tf_op jit(solution)/shard_map/all_gather | solution.py:58
  28.3 0.0 copy-start.1
  28.3 1.5 %copy.15 = bf16[256,2048]{1,0:T(8,128)(2,1)S(1)} copy(bf16[256,2048]{0,1:T(8,128)(2,1)} %bitcast.110) | data formatting | bytes 2097152 | tf_op jit(solution)/shard_map/dot_general | solution.py:62
  29.9 0.0 copy-done
  29.9 0.5 multiply_reduce_fusion.1
  30.3 0.0 copy-done.1
  30.3 0.1 multiply_multiply_fusion.1
  30.5 0.1 copy.16
  30.6 16.0 %all-gather.7.cloned.1.call-done = bf16[2048,256]{1,0:T(8,128)(2,1)} async-done(((bf16[512,256]{1,0:T(8,128)(2,1)}), bf16[2048,256]{1,0:T(8,128)(2,1)}) %all-gather.7.cloned.1.call-update) | async-done | bytes 1048592 | tf_op jit(solution)/shard_map/all_gather | solution.py:59
  46.6 1.6 %fusion.15 = bf16[160,1,256]{2,0,1:T(8,128)(2,1)S(1)} fusion(bf16[2048,256]{1,0:T(8,128)(2,1)} %all-gather.7.cloned.1.call-done, bf16[1,160,2048]{2,1,0:T(8,128)(2,1)S(1)} %copy-done), kind=kOutput, calls=%fused_computation.22 | convolution fusion | flops 167813120 | bytes 1785856 | tf_op jit(solution)/shard_map/dot_general | solution.py:62
  48.2 18.1 %all_gather.17 = bf16[640,2,256]{2,0,1:T(8,128)(2,1)S(1)} all-gather(bf16[160,2,256]{2,0,1:T(8,128)(2,1)S(1)} %pad_maximum_fusion), channel_id=1, replica_groups=mesh['grp'=2,'sp'=4,'dp'=4] {'sp'}, dimensions={0}, use_global_device_ids=true | all-gather | bytes 819200 | tf_op jit(solution)/shard_map/all_gather | solution.py:76
  66.4 0.2 copy.18
  66.6 0.2 copy.17
  66.8 15.9 %all-gather.9.cloned.1.call-done = bf16[2048,1024]{1,0:T(8,128)(2,1)} async-done(((bf16[512,1024]{1,0:T(8,128)(2,1)}), bf16[2048,1024]{1,0:T(8,128)(2,1)}) %all-gather.9.cloned.1.call-update) | async-done | bytes 4194320 | tf_op jit(solution)/shard_map/all_gather | solution.py:57
  82.7 6.5 %copy.19 = bf16[1024,2048]{1,0:T(8,128)(2,1)} copy(bf16[1024,2048]{0,1:T(8,128)(2,1)} %bitcast.106) | data formatting | bytes 8388608 | tf_op jit(solution)/shard_map/dot_general | solution.py:62
  89.2 0.0 copy-start.2
  89.2 3.9 %multiply_reduce_fusion = (f32[160,16]{0,1:T(8,128)S(1)}, f32[160,16,64]{0,2,1:T(8,128)S(1)}) fusion(bf16[16,64,2048]{2,1,0:T(8,128)(2,1)} %bitcast.107, bf16[1,160,2048]{2,1,0:T(8,128)(2,1)S(1)} %copy-done), kind=kOutput, calls=%fused_computation.24 | convolution fusion | flops 671413760 | bytes 5515264 | tf_op jit(solution)/shard_map/dot_general | solution.py:62
  93.1 0.0 copy-done.2
  93.1 0.2 multiply_multiply_fusion
  93.3 0.2 subtract_convert_fusion
  93.5 0.1 maximum_bitcast_fusion
  93.6 7.3 %while.10 = (s32[]{:T(128)}, bf16[4,160,256]{1,2,0:T(8,128)(2,1)S(1)}, bf16[4,640,1,64]{1,3,2,0:T(8,128)(2,1)S(1)}, bf16[4,640,1,64]{1,3,2,0:T(8,128)(2,1)S(1)},...) while((s32[]{:T(128)}, bf16[4,160,256]{1,2,0:T(8,128)(2,1)S(1)}, bf16[4,640,1,64]{1,3,2,0:T(8,128)(2,1)S(1)}, ...), condition=%wide.region_5.6_spmd, body=%wide.region_2.5_spmd.sunk | while | flops 108583680 | bytes 5571157 | solution.py:86
  93.6 0.6 bitcast_reduce_fusion.2
  94.2 0.5 fusion.37
  94.7 0.6 convolution_convert_fusion.4
  95.4 0.6 bitcast_reduce_fusion.2
  96.0 0.5 fusion.37
  96.5 0.6 convolution_convert_fusion.4
  97.2 0.6 bitcast_reduce_fusion.2
  97.8 0.5 fusion.37
  98.4 0.6 convolution_convert_fusion.4
  99.0 0.6 bitcast_reduce_fusion.2
  99.7 0.5 fusion.37
  100.2 0.6 convolution_convert_fusion.4
  100.9 17.7 %all-gather.11.cloned.1.call-done = bf16[1024,2048]{1,0:T(8,128)(2,1)} async-done(((bf16[1024,512]{1,0:T(8,128)(2,1)}), bf16[1024,2048]{1,0:T(8,128)(2,1)}) %all-gather.11.cloned.1.call-update) | async-done | bytes 4194320 | tf_op jit(solution)/shard_map/all_gather | solution.py:90
  118.6 3.9 %fusion.14 = bf16[1,160,2048]{2,1,0:T(8,128)(2,1)} fusion(bf16[160,1024]{0,1:T(8,128)(2,1)S(1)} %bitcast.115, bf16[1024,2048]{1,0:T(8,128)(2,1)} %all-gather.11.cloned.1.call-done), kind=kOutput, calls=%fused_computation.20 | convolution fusion | flops 671416320 | bytes 5177344 | tf_op jit(solution)/shard_map/dot_general | solution.py:88
  (13 shorter events, 0.2 us)
Async XLA Ops:
  6.5 23.3 %copy-start = (bf16[1,160,2048]{2,1,0:T(8,128)(2,1)S(1)}, bf16[1,160,2048]{2,1,0:T(8,128)(2,1)}, u32[]{:S(2)}) copy-start(bf16[1,160,2048]{2,1,0:T(8,128)(2,1)} %param.9) | copy-start | bytes 1966084
  6.5 21.8 %all-gather.5.cloned.1.call-start = ((), (), s32[]{:S(2)}) async-start(), calls=%async_computation | async-start | bytes 1310720 | tf_op jit(solution)/shard_map/all_gather | solution.py:58
  7.3 39.4 %all-gather.7.cloned.1.call-start = ((), (), s32[]{:S(2)}) async-start(), calls=%async_computation.1 | async-start | bytes 1310720 | tf_op jit(solution)/shard_map/all_gather | solution.py:59
  8.0 74.7 %all-gather.9.cloned.1.call-start = ((), (), s32[]{:S(2)}) async-start(), calls=%async_computation.2 | async-start | bytes 5242880 | tf_op jit(solution)/shard_map/all_gather | solution.py:57
  8.7 109.9 %all-gather.11.cloned.1.call-start = ((), (), s32[]{:S(2)}) async-start(), calls=%async_computation.3 | async-start | bytes 5242880 | tf_op jit(solution)/shard_map/all_gather | solution.py:90
  28.3 2.0 %copy-start.1 = (f32[64]{0:T(128)S(1)}, f32[64]{0:T(128)}, u32[]{:S(2)}) copy-start(f32[64]{0:T(128)} %param.15) | copy-start | bytes 772
  89.2 3.9 %copy-start.2 = (f32[64]{0:T(128)S(1)}, f32[64]{0:T(128)}, u32[]{:S(2)}) copy-start(f32[64]{0:T(128)} %param.14) | copy-start | bytes 772
Sparse Core Ops, SparseCore 0:
  8.9 19.4 all-gather.4
  29.9 16.6 all-gather.6
  48.2 34.4 all-gather.8
  84.1 34.4 all-gather.10
where the time goes:
time: 129 us
  waiting for transfers between devices  71 us (55%)
  blocking collectives  18.1 us (14%)
  matrix products  14.8 us (11%)
  between operations  13.3 us (10%)
  local copies, waits for them, and re-layouts  8.62 us (7%)
  other arithmetic  2.96 us (2%)
    all_gather x1, waiting for transfers between devices, shards(): lax.all_gather(key_weight, 'dp', axis=0, tiled=True)  18.8 us
    all_gather x1, blocking collectives, shards(): whole_kv = lax.all_gather(kv_pair, 'sp', axis=0, tiled=True)  18.1 us
    all_gather x1, waiting for transfers between devices, shards(): lax.all_gather(out_weight, 'dp', axis=1, tiled=True)  17.7 us
    all_gather x1, waiting for transfers between devices, shards(): lax.all_gather(value_weight, 'dp', axis=0, tiled=True)  16 us
    all_gather x1, waiting for transfers between devices, shards(): lax.all_gather(query_weight, 'dp', axis=0, tiled=True)  15.9 us
    dot_general x2, local copies, waits for them, and re-layouts, shards(): jnp.dot(local_rows, piece, preferred_element_type=jnp.float32)  7.99 us
    dot_general x3, matrix products, shards(): jnp.dot(local_rows, piece, preferred_element_type=jnp.float32)  5.89 us
    dot_general x1, matrix products, shards(): jnp.dot(attended, lax.all_gather(out_weight, 'dp', axis=1, tiled=True), p...  3.9 us
  transfers between devices with their start and end apart: 4, of which 4 were waited for; matrix products, arithmetic and copies ran while one was open for 17% of the time, Pallas kernels for 0%

commit v1 on v0

v1 whole, which is shorter than its diff:
```python
import functools

import jax
import jax.numpy as jnp
from jax import lax
from jax.experimental import pallas as pl
from jax.experimental.pallas import tpu as pltpu
from jax.sharding import PartitionSpec as P

HEADS = 16
KV_HEADS = 4
HEAD_DIM = 64
GRID_W = 64
LANES = 128

theta_base = 10000.0
norm_eps = 1e-06

BF = jnp.bfloat16
F32 = jnp.float32
MESH = pl.DeviceIdType.MESH


def rotary_tables(positions):
    quarter = HEAD_DIM // 4
    inverse = theta_base ** (-jnp.arange(quarter, dtype=F32) / quarter)
    grid_rows = (positions // GRID_W).astype(F32)
    grid_cols = (positions % GRID_W).astype(F32)
    angles = jnp.concatenate([grid_rows[:, None] * inverse, grid_cols[:, None] * inverse], axis=-1)
    return (jnp.cos(angles), jnp.sin(angles))


def dot(a, b):
    return jnp.dot(a, b, preferred_element_type=F32)


def kernel(n, groups, seqs, cuts, tok, wk, wv, wq, wo, cos, sin, gq, gk, out,
           fk, fv, fq, fo, kv, acc_k, acc_v, acc_q, qs, k2, v2, att,
           xs, xr, ys, yr, os_, or_, cxs, cxr, cys, cyr, zs, zr):
    d = lax.axis_index("dp")
    g = lax.axis_index("grp")
    s = lax.axis_index("sp")
    chips = n // 2
    mate = d + 1 - 2 * lax.rem(d, 2)
    own = (wk, wv, wq, wo)
    full = (fk, fv, fq, fo)
    rows = tok.shape[0]

    def hop(j):
        return lax.rem(d + 2 * j, n)

    def back(dev, j):
        return lax.rem(dev + n - 2 * j, n)

    def color(i):
        return lax.rem(g + groups - i, groups)

    barrier = pltpu.get_barrier_semaphore()
    for j in range(1, chips):
        pl.semaphore_signal(barrier, inc=1, device_id={"dp": hop(j)}, device_id_type=MESH)
    for i in range(1, groups):
        pl.semaphore_signal(barrier, inc=1, device_id={"grp": lax.rem(g + i, groups)}, device_id_type=MESH)
    for i in range(1, seqs):
        pl.semaphore_signal(barrier, inc=1, device_id={"sp": lax.rem(s + i, seqs)}, device_id_type=MESH)
    pl.semaphore_signal(barrier, inc=1, device_id={"dp": mate}, device_id_type=MESH)
    pl.semaphore_wait(barrier, chips - 1 + groups - 1 + seqs - 1 + 1)

    sent = []

    def send(src, dst, ssem, rsem, where):
        copy = pltpu.make_async_remote_copy(
            src_ref=src, dst_ref=dst, send_sem=ssem, recv_sem=rsem, device_id=where, device_id_type=MESH)
        copy.start()
        sent.append(copy)

    def arrive(dst, ssem, rsem):
        pltpu.make_async_remote_copy(
            src_ref=dst, dst_ref=dst, send_sem=ssem, recv_sem=rsem,
            device_id={"dp": mate}, device_id_type=MESH).wait_recv()

    pieces = [(kind, cut) for kind in range(4) for cut in range(cuts[kind])]

    def span(p, which):
        kind, cut = pieces[p]
        size = own[kind].shape[0] // groups // cuts[kind]
        start = which * (own[kind].shape[0] // groups) + cut * size
        return pl.ds(pl.multiple_of(start, 16), size)

    for p in range(len(pieces)):
        kind = pieces[p][0]
        for j in range(1, chips):
            part = span(p, g)
            send(own[kind].at[part], full[kind].at[d, part], xs.at[j - 1, p], xr.at[j - 1, p], {"dp": hop(j)})
    for kind in range(4):
        send(own[kind], full[kind].at[d], os_.at[kind], or_.at[kind], {"dp": mate})

    def step_x(p):
        kind = pieces[p][0]
        part = span(p, g)
        for j in range(1, chips):
            owner = back(d, j)
            here = full[kind].at[owner, part]
            arrive(here, xs.at[j - 1, p], xr.at[j - 1, p])
            for i in range(1, groups):
                send(here, here, ys.at[j - 1, i - 1, p], yr.at[j - 1, i - 1, p],
                     {"grp": lax.rem(g + i, groups)})
            send(here, here, cxs.at[j - 1, p], cxr.at[j - 1, p], {"dp": mate})

    def step_y(p):
        kind = pieces[p][0]
        for j in range(1, chips):
            owner = back(d, j)
            for i in range(1, groups):
                here = full[kind].at[owner, span(p, color(i))]
                arrive(here, ys.at[j - 1, i - 1, p], yr.at[j - 1, i - 1, p])
                send(here, here, cys.at[j - 1, i - 1, p], cyr.at[j - 1, i - 1, p], {"dp": mate})

    def step_own(kind):
        arrive(full[kind].at[mate], os_.at[kind], or_.at[kind])

    def step_c(p):
        kind = pieces[p][0]
        for j in range(1, chips):
            owner = back(mate, j)
            arrive(full[kind].at[owner, span(p, g)], cxs.at[j - 1, p], cxr.at[j - 1, p])
            for i in range(1, groups):
                arrive(full[kind].at[owner, span(p, color(i))],
                       cys.at[j - 1, i - 1, p], cyr.at[j - 1, i - 1, p])

    depth = wq.shape[0]

    def columns(owner):
        return pl.ds(pl.multiple_of(owner * depth, LANES), depth)

    def first(acc, ref):
        acc[...] = dot(tok[:, columns(d)], ref[...])

    def more(acc, ref, owner):
        acc[...] += dot(tok[:, columns(owner)], ref[owner])

    first(acc_k, wk)
    first(acc_v, wv)
    first(acc_q, wq)

    lane = lax.broadcasted_iota(jnp.int32, (rows, LANES), 1)
    low_half = lax.rem(lane, HEAD_DIM) < HEAD_DIM // 2
    low_head = lane < HEAD_DIM
    square_r = lax.broadcasted_iota(jnp.int32, (LANES, LANES), 0)
    square_c = lax.broadcasted_iota(jnp.int32, (LANES, LANES), 1)
    same_head = jnp.where(square_r // HEAD_DIM == square_c // HEAD_DIM, 1.0, 0.0).astype(BF)

    def norm_rotate(raw, gain):
        sq = raw * raw
        high = sq.astype(BF)
        low = (sq - high.astype(F32)).astype(BF)
        total = dot(high, same_head) + dot(low, same_head)
        scaled = raw * lax.rsqrt(total * (1.0 / HEAD_DIM) + norm_eps) * gain
        other = jnp.where(low_half, pltpu.roll(scaled, LANES - HEAD_DIM // 2, 1),
                          pltpu.roll(scaled, HEAD_DIM // 2, 1))
        return scaled * cos[...] + other * sin[...]

    others = [(d, j) for j in range(1, chips)] + [(mate, j) for j in range(1, chips)]

    def finish_kv():
        for acc, kind in ((acc_k, 0), (acc_v, 1)):
            for p in range(len(pieces)):
                if pieces[p][0] == kind:
                    step_c(p)
            for dev, j in others:
                more(acc, full[kind], back(dev, j))
        width = wk.shape[1]
        for t in range(width // LANES):
            cols = pl.ds(t * LANES, LANES)
            kv[s, :, cols] = norm_rotate(acc_k[:, cols], gk[...]).astype(BF)
        kv[s, :, pl.ds(width, width)] = acc_v[...].astype(BF)
        for i in range(1, seqs):
            send(kv.at[s], kv.at[s], zs.at[i - 1], zr.at[i - 1], {"sp": lax.rem(s + i, seqs)})

    def finish_q():
        for p in range(len(pieces)):
            if pieces[p][0] == 2:
                step_c(p)
        for dev, j in others:
            more(acc_q, fq, back(dev, j))
        for t in range(wq.shape[1] // LANES):
            turned = norm_rotate(acc_q[:, pl.ds(t * LANES, LANES)], gq[...]).astype(BF).astype(F32)
            turned = turned * HEAD_DIM ** (-0.5)
            qs[t, pl.ds(0, rows), :] = jnp.where(low_head, turned, 0.0).astype(BF)
            qs[t, pl.ds(rows, rows), :] = jnp.where(low_head, 0.0, turned).astype(BF)

    def gather_kv():
        for i in range(1, seqs):
            arrive(kv.at[lax.rem(s + seqs - i, seqs)], zs.at[i - 1], zr.at[i - 1])
        width = wk.shape[1]
        for h in range(KV_HEADS):
            offset = (h % 2) * HEAD_DIM
            twice = jnp.where(square_r == offset + lax.rem(square_c, HEAD_DIM), 1.0, 0.0).astype(BF)
            base = (h // 2) * LANES
            for src, dst in ((base, k2), (width + base, v2)):
                block = kv[:, :, pl.ds(src, LANES)].reshape(seqs * rows, LANES)
                dst[h] = dot(block, twice).astype(BF)

    tiles = wq.shape[1] // LANES

    def attend(lo, hi):
        def body(t, carry):
            h = t // (tiles // KV_HEADS)
            scores = lax.dot_general(qs[t], k2[h], (((1,), (1,)), ((), ())), preferred_element_type=F32)
            top = jnp.max(scores, axis=-1, keepdims=True)
            weights = jnp.exp(scores - top)
            inverse = 1.0 / jnp.sum(weights, axis=-1, keepdims=True)
            mixed = dot((weights * inverse).astype(BF), v2[h])
            att[:, pl.ds(pl.multiple_of(t * LANES, LANES), LANES)] = jnp.where(
                low_head, mixed[:rows], mixed[rows:]).astype(BF)
            return carry
        lax.fori_loop(lo, hi, body, 0)

    def project(ref, owner):
        width = wo.shape[1]
        out[:, pl.ds(pl.multiple_of(owner * width, LANES), width)] = dot(att[...], ref).astype(BF)

    total = len(pieces)
    kv_end = cuts[0] + cuts[1]
    q_end = kv_end + cuts[2]
    left = cuts[3]
    done = 0
    for p in range(total):
        step_x(p)
        if p >= 1:
            step_y(p - 1)
        if p == 1:
            step_own(0)
            more(acc_k, fk, mate)
            step_own(1)
            more(acc_v, fv, mate)
        if p == kv_end:
            finish_kv()
            step_own(2)
            more(acc_q, fq, mate)
        if p == q_end:
            finish_q()
        if p > q_end:
            if p == q_end + 1:
                gather_kv()
            upto = tiles * (p - q_end) // left
            attend(done, upto)
            done = upto
    step_y(total - 1)
    attend(done, tiles)
    project(wo[...], d)
    step_own(3)
    project(fo[mate], mate)
    for j in range(1, chips):
        project(fo[back(d, j)], back(d, j))
    for p in range(q_end, total):
        step_c(p)
    for j in range(1, chips):
        project(fo[back(mate, j)], back(mate, j))
    for copy in sent:
        copy.wait_send()


def shards(n, groups, seqs, tokens, query_weight, key_weight, value_weight, out_weight, query_gain, key_gain):
    rows, width = tokens.shape[1], tokens.shape[2]
    local = tokens.reshape(rows, width)
    positions = lax.axis_index("sp") * rows + jnp.arange(rows, dtype=jnp.int32)
    cosine, sine = rotary_tables(positions)
    cos = jnp.concatenate([cosine] * 4, axis=1)
    sin = jnp.concatenate([-sine, sine] * 2, axis=1)
    gq = jnp.tile(query_gain, 2).reshape(1, LANES)
    gk = jnp.tile(key_gain, 2).reshape(1, LANES)
    cuts = (1, 1, 4, 4)
    count = sum(cuts)
    chips = n // 2
    kvw, qw = key_weight.shape[1], query_weight.shape[1]
    length = rows * seqs
    dma = pltpu.SemaphoreType.DMA
    vmem = pl.BlockSpec(memory_space=pltpu.VMEM)
    result = pl.pallas_call(
        functools.partial(kernel, n, groups, seqs, cuts),
        out_shape=jax.ShapeDtypeStruct((rows, width), BF),
        in_specs=[vmem] * 9,
        out_specs=vmem,
        scratch_shapes=[
            pltpu.VMEM((n,) + key_weight.shape, BF),
            pltpu.VMEM((n,) + value_weight.shape, BF),
            pltpu.VMEM((n,) + query_weight.shape, BF),
            pltpu.VMEM((n,) + out_weight.shape, BF),
            pltpu.VMEM((seqs, rows, 2 * kvw), BF),
            pltpu.VMEM((rows, kvw), F32),
            pltpu.VMEM((rows, kvw), F32),
            pltpu.VMEM((rows, qw), F32),
            pltpu.VMEM((qw // LANES, 2 * rows, LANES), BF),
            pltpu.VMEM((KV_HEADS, length, LANES), BF),
            pltpu.VMEM((KV_HEADS, length, LANES), BF),
            pltpu.VMEM((rows, qw), BF),
            dma((chips - 1, count)), dma((chips - 1, count)),
            dma((chips - 1, groups - 1, count)), dma((chips - 1, groups - 1, count)),
            dma((4,)), dma((4,)),
            dma((chips - 1, count)), dma((chips - 1, count)),
            dma((chips - 1, groups - 1, count)), dma((chips - 1, groups - 1, count)),
            dma((seqs - 1,)), dma((seqs - 1,)),
        ],
        compiler_params=pltpu.CompilerParams(
            collective_id=0, has_side_effects=True, vmem_limit_bytes=60 * 2 ** 20),
    )(local, key_weight, value_weight, query_weight, out_weight, cos, sin, gq, gk)
    return result.reshape(1, rows, width)


def solution(mesh):
    in_specs = (
        P(("grp", "dp"), "sp", None),
        P("dp", None),
        P("dp", None),
        P("dp", None),
        P(None, "dp"),
        P(),
        P(),
    )
    out_specs = P(("grp", "dp"), "sp", None)
    body = functools.partial(shards, mesh.shape["dp"], mesh.shape["grp"], mesh.shape["sp"])
    return jax.shard_map(body, mesh=mesh, in_specs=in_specs, out_specs=out_specs, check_vma=False)
```

time: 129 us -> 56.8 us (0.44)
  waiting for transfers between devices: 71 us -> 0 us
  Pallas kernels: 0 us -> 50.6 us
  blocking collectives: 18.1 us -> 0 us
  matrix products: 14.8 us -> 0 us
  between operations: 13.3 us -> 0.03 us
  local copies, waits for them, and re-layouts: 8.62 us -> 4.14 us
    all_gather x4 -> x0, waiting for transfers between devices: 68.4 us -> none  [the longest x1 18.8 us: shards(): lax.all_gather(key_weight, 'dp', axis=0, tiled=True)]
    pallas_call x0 -> x1, Pallas kernels: none -> 50.6 us  [shards(): pl.pallas_call(functools.partial(kernel, n, groups, seqs, cuts), out_shap...]
    all_gather x1 -> x0, blocking collectives: 18.1 us -> none  [shards(): whole_kv = lax.all_gather(kv_pair, 'sp', axis=0, tiled=True)]
    dot_general x12 -> x0, matrix products: 14.8 us -> none  [the longest x3 5.89 us: shards(): jnp.dot(local_rows, piece, preferred_element_type=jnp.float32)]
    dot_general x2 -> x0, local copies, waits for them, and re-layouts: 7.99 us -> none  [shards(): jnp.dot(local_rows, piece, preferred_element_type=jnp.float32)]
    unnamed x6 -> x5, local copies, waits for them, and re-layouts: 0.01 us -> 2.67 us
    unnamed x4 -> x0, waiting for transfers between devices: 2.61 us -> none
    reduce_sum x4 -> x0, other arithmetic: 2.07 us -> none  [attend_block(): jnp.sum(weights, axis=-1, keepdims=True)]
  transfers between devices with their start and end apart: 4 -> 0, of which waited for: 4 -> 0; matrix products, arithmetic and copies ran while one was open for 17% -> 0% of each run, Pallas kernels for 0% -> 0%
where the time goes in v1:
time: 56.8 us; the launch traced here: 56.6 us
  Pallas kernels  50.6 us (89%)
  local copies, waits for them, and re-layouts  4.14 us (7%)
  other arithmetic  1.77 us (3%)
    pallas_call x1, Pallas kernels, shards(): pl.pallas_call(functools.partial(kernel, n, groups, seqs, cuts), out_shap...  50.6 us
    unnamed x5, local copies, waits for them, and re-layouts  2.67 us

profile of v1, /device:TPU:0, one launch (start us, length us, event | category | flops | bytes accessed | tf_op | source)
XLA Modules:
  0.0 56.6 jit_solution(12564533809170342703)
XLA Ops:
  0.0 0.0 copy-start
  0.0 0.6 %copy-done = f32[64]{0:T(128)S(1)} copy-done((f32[64]{0:T(128)S(1)}, f32[64]{0:T(128)}, u32[]{:S(2)}) %copy-start) | copy-done | bytes 280
  0.7 0.0 copy-start.1
  0.7 0.6 %reshape_tile.6.gq = f32[1,128]{1,0:T(1,128)} reshape(f32[2,64]{1,0:T(2,128)S(1)} %tile.4) | data formatting | bytes 1024 | tf_op jit(solution)/shard_map/reshape;tile | solution.py:270
  1.3 0.0 copy-done.1
  1.3 0.7 %reshape_tile.7.gk = f32[1,128]{1,0:T(1,128)} reshape(f32[2,64]{1,0:T(2,128)S(1)} %tile.5) | data formatting | bytes 1024 | tf_op jit(solution)/shard_map/reshape;tile | solution.py:271
  2.0 0.1 broadcast_multiply_fusion.1
  2.1 0.1 fusion
  2.2 0.1 copy.14
  2.3 0.8 %pad_maximum_fusion.1.sin = f32[160,128]{1,0:T(8,128)} fusion(f32[160,32]{1,0:T(8,128)S(1)} %copy.14, f32[160,32]{1,0:T(8,128)S(1)} %neg.13), kind=kLoop, calls=%fused_computation.1 | loop fusion | flops 61440 | bytes 122880 | tf_op jit(solution)/shard_map/concatenate | solution.py:269
  3.1 0.1 copy.10
  3.2 0.8 %pad_maximum_fusion.cos = f32[160,128]{1,0:T(8,128)} fusion(f32[160,32]{1,0:T(8,128)S(1)} %copy.10), kind=kLoop, calls=%fused_computation | loop fusion | flops 61440 | bytes 102400 | tf_op jit(solution)/shard_map/concatenate | solution.py:268
  3.9 50.6 %shard_map.73 = bf16[160,2048]{1,0:T(8,128)(2,1)} custom-call(bf16[160,2048]{1,0:T(8,128)(2,1)} %bitcast.3, bf16[512,256]{1,0:T(8,128)(2,1)} %wk.1, bf16[512,256]{1,0:T(8,128)(2,1)} %wv.1, bf16[512,1024]{1,0:T(8,128)(2,1)} %wq.1, bf16[1024,512]{1,0:T(8,128)(2,1)} %wo.1, f32[160,128]{1,0:T(8,128)} %pad_maximum_fusion.cos, f32[160,128]{1,0:T(8,128)} %pad_maximum_fusion.1.sin, ...), custom_call_target="tpu_custom_call" | custom-call | tf_op jit(solution)/shard_map/pallas_call | solution.py:279
  54.6 2.0 %copy.18 = bf16[1,160,2048]{2,1,0:T(8,128)(2,1)} copy(bf16[1,160,2048]{2,1,0:T(8,128)(2,1)} %bitcast.2) | data formatting | bytes 1310720
  (5 shorter events, 0.0 us)
Async XLA Ops:
  0.0 0.7 %copy-start = (f32[64]{0:T(128)S(1)}, f32[64]{0:T(128)}, u32[]{:S(2)}) copy-start(f32[64]{0:T(128)} %param.12) | copy-start | bytes 772
  0.7 0.7 %copy-start.1 = (f32[64]{0:T(128)S(1)}, f32[64]{0:T(128)}, u32[]{:S(2)}) copy-start(f32[64]{0:T(128)} %param.13) | copy-start | bytes 772

commit v2 on v1

v2 whole, which is shorter than its diff:
```python
import functools
import math

import jax
import jax.numpy as jnp
from jax import lax
from jax.experimental import pallas as pl
from jax.experimental.pallas import tpu as pltpu
from jax.sharding import PartitionSpec as P

HEADS = 16
KV_HEADS = 4
HEAD_DIM = 64
GRID_W = 64
LANES = 128

theta_base = 10000.0
norm_eps = 1e-06

BF = jnp.bfloat16
F32 = jnp.float32
MESH = pl.DeviceIdType.MESH


def rotary_tables(start, rows):
    quarter = HEAD_DIM // 4
    lane = lax.broadcasted_iota(jnp.int32, (rows, LANES), 1)
    position = start + lax.broadcasted_iota(jnp.int32, (rows, LANES), 0)
    step = lax.rem(lane, quarter).astype(F32)
    inverse = jnp.exp(step * (-math.log(theta_base) / quarter))
    grid_row = lax.div(position, GRID_W)
    grid_col = lax.rem(position, GRID_W)
    place = jnp.where(lax.rem(lane, 2 * quarter) < quarter, grid_row, grid_col).astype(F32)
    angles = place * inverse
    sine = jnp.sin(angles)
    return jnp.cos(angles), jnp.where(lax.rem(lane, HEAD_DIM) < HEAD_DIM // 2, -sine, sine)


def dot(a, b):
    return jnp.dot(a, b, preferred_element_type=F32)


def kernel(n, groups, seqs, cuts, order, tok, wk, wv, wq, wo, gq, gk, out,
           fk, fv, fq, fo, cos, sin, kv, acc_k, acc_v, acc_q, qs, k2, v2, att,
           xs, xr, ys, yr, ps, pr, os_, or_, cxs, cxr, zs, zr):
    d = lax.axis_index("dp")
    g = lax.axis_index("grp")
    s = lax.axis_index("sp")
    chips = n // 2
    mate = d + 1 - 2 * lax.rem(d, 2)
    own = (wk, wv, wq, wo)
    full = (fk, fv, fq, fo)
    rows = tok.shape[0]

    def hop(j):
        return lax.rem(d + 2 * j, n)

    def back(dev, j):
        return lax.rem(dev + n - 2 * j, n)

    def other(i):
        return i + 1 - 2 * lax.rem(i, 2)

    e = lax.rem(s, 2)
    colors = (2 * g + e, 2 * other(g) + e, 2 * g + other(e), 2 * other(g) + other(e))

    barrier = pltpu.get_barrier_semaphore()
    for j in range(1, chips):
        pl.semaphore_signal(barrier, inc=1, device_id={"dp": hop(j)}, device_id_type=MESH)
    for i in range(1, groups):
        pl.semaphore_signal(barrier, inc=1, device_id={"grp": lax.rem(g + i, groups)}, device_id_type=MESH)
    for i in range(1, seqs):
        pl.semaphore_signal(barrier, inc=1, device_id={"sp": lax.rem(s + i, seqs)}, device_id_type=MESH)
    pl.semaphore_signal(barrier, inc=1, device_id={"dp": mate}, device_id_type=MESH)
    pl.semaphore_wait(barrier, chips - 1 + groups - 1 + seqs - 1 + 1)

    sent = []

    def send(src, dst, ssem, rsem, where):
        copy = pltpu.make_async_remote_copy(
            src_ref=src, dst_ref=dst, send_sem=ssem, recv_sem=rsem, device_id=where, device_id_type=MESH)
        copy.start()
        sent.append(copy)

    def arrive(dst, ssem, rsem):
        pltpu.make_async_remote_copy(
            src_ref=dst, dst_ref=dst, send_sem=ssem, recv_sem=rsem,
            device_id={"dp": mate}, device_id_type=MESH).wait_recv()

    pieces = [(kind, cut) for kind in range(4) for cut in range(cuts[kind])]

    def block(ref, p, color):
        kind, cut = pieces[p]
        quarter = own[kind].shape[0] // 4
        size = quarter // cuts[kind]
        start = color * quarter + cut * size
        return ref.at[pl.ds(pl.multiple_of(start, 16), size)]

    def held(owner, p, rel):
        return block(full[pieces[p][0]].at[owner], p, colors[rel])

    ahead = 4

    def x_copy(index, j):
        p, rel = order[index]
        return pltpu.make_async_remote_copy(
            src_ref=block(own[pieces[p][0]], p, colors[rel]), dst_ref=held(d, p, rel),
            send_sem=xs.at[j - 1, rel, p], recv_sem=xr.at[j - 1, rel, p],
            device_id={"dp": hop(j)}, device_id_type=MESH)

    for index in range(min(ahead, len(order))):
        for j in range(1, chips):
            x_copy(index, j).start()
    for kind in range(4):
        send(own[kind], full[kind].at[d], os_.at[kind], or_.at[kind], {"dp": mate})

    def to_mate(here, j, rel, p):
        send(here, here, cxs.at[j - 1, rel, p], cxr.at[j - 1, rel, p], {"dp": mate})

    def step_x(p, rel):
        index = order.index((p, rel))
        for j in range(1, chips):
            here = held(back(d, j), p, rel)
            arrive(here, xs.at[j - 1, rel, p], xr.at[j - 1, rel, p])
            if rel != 3:
                send(here, here, ys.at[j - 1, rel // 2, p], yr.at[j - 1, rel // 2, p], {"grp": other(g)})
            if rel == 0 and (p, 2) not in order:
                send(here, here, ps.at[j - 1, p], pr.at[j - 1, p], {"sp": other(s)})
            to_mate(here, j, rel, p)
        for j in range(1, chips):
            x_copy(index, j).wait_send()
            if index + ahead < len(order):
                x_copy(index + ahead, j).start()

    def step_y(p, rel=1):
        for j in range(1, chips):
            here = held(back(d, j), p, rel)
            arrive(here, ys.at[j - 1, rel // 3, p], yr.at[j - 1, rel // 3, p])
            to_mate(here, j, rel, p)

    def step_z(p):
        for j in range(1, chips):
            here = held(back(d, j), p, 2)
            arrive(here, ps.at[j - 1, p], pr.at[j - 1, p])
            if (p, 3) not in order:
                send(here, here, ys.at[j - 1, 1, p], yr.at[j - 1, 1, p], {"grp": other(g)})
            to_mate(here, j, 2, p)

    def step_own(kind):
        arrive(full[kind].at[mate], os_.at[kind], or_.at[kind])

    def step_c(p):
        for j in range(1, chips):
            for rel in range(4):
                arrive(held(back(mate, j), p, rel), cxs.at[j - 1, rel, p], cxr.at[j - 1, rel, p])

    depth = wq.shape[0]

    def columns(owner):
        return pl.ds(pl.multiple_of(owner * depth, LANES), depth)

    def first(acc, ref):
        acc[...] = dot(tok[:, columns(d)], ref[...])

    def more(acc, ref, owner):
        acc[...] += dot(tok[:, columns(owner)], ref[owner])

    cos[...], sin[...] = rotary_tables(s * rows, rows)
    first(acc_k, wk)
    first(acc_v, wv)
    first(acc_q, wq)

    lane = lax.broadcasted_iota(jnp.int32, (rows, LANES), 1)
    low_half = lax.rem(lane, HEAD_DIM) < HEAD_DIM // 2
    low_head = lane < HEAD_DIM
    square_r = lax.broadcasted_iota(jnp.int32, (LANES, LANES), 0)
    square_c = lax.broadcasted_iota(jnp.int32, (LANES, LANES), 1)
    same_head = jnp.where(square_r // HEAD_DIM == square_c // HEAD_DIM, 1.0, 0.0).astype(BF)

    gain_k = jnp.concatenate([gk[...]] * 2, axis=1)
    gain_q = jnp.concatenate([gq[...]] * 2, axis=1)

    def norm_rotate(raw, gain):
        sq = raw * raw
        high = sq.astype(BF)
        low = (sq - high.astype(F32)).astype(BF)
        total = dot(high, same_head) + dot(low, same_head)
        scaled = raw * lax.rsqrt(total * (1.0 / HEAD_DIM) + norm_eps) * gain
        other = jnp.where(low_half, pltpu.roll(scaled, LANES - HEAD_DIM // 2, 1),
                          pltpu.roll(scaled, HEAD_DIM // 2, 1))
        return scaled * cos[...] + other * sin[...]

    others = [(d, j) for j in range(1, chips)] + [(mate, j) for j in range(1, chips)]

    held_back = []

    def relay(k):
        for way in range(2):
            sign = 2 * way - 1
            source, target = s + sign * k, s - sign
            here = (source >= 0) & (source < seqs)
            there = here & (target >= 0) & (target < seqs)
            slot = jnp.clip(source, 0, seqs - 1)
            goal = jnp.clip(target, 0, seqs - 1)
            width = kv.shape[2] // 2
            for half in range(2):
                ref = kv.at[slot, :, pl.ds(half * width, width)]
                if k > 0:
                    @pl.when(here)
                    def _():
                        arrive(ref, zs.at[way, half, k - 1], zr.at[way, half, k - 1])
                if k < seqs - 1:
                    copy = pltpu.make_async_remote_copy(
                        src_ref=ref, dst_ref=ref, send_sem=zs.at[way, half, k], recv_sem=zr.at[way, half, k],
                        device_id={"sp": goal}, device_id_type=MESH)
                    pl.when(there)(copy.start)
                    held_back.append((there, copy))

    def finish_kv():
        for acc, kind in ((acc_k, 0), (acc_v, 1)):
            for p in range(len(pieces)):
                if pieces[p][0] == kind:
                    step_c(p)
            for dev, j in others:
                more(acc, full[kind], back(dev, j))
        width = wk.shape[1]
        for t in range(width // LANES):
            cols = pl.ds(t * LANES, LANES)
            kv[s, :, cols] = norm_rotate(acc_k[:, cols], gain_k).astype(BF)
        kv[s, :, pl.ds(width, width)] = acc_v[...].astype(BF)
        relay(0)

    def finish_q():
        for p in range(len(pieces)):
            if pieces[p][0] == 2:
                step_c(p)
        for dev, j in others:
            more(acc_q, fq, back(dev, j))
        for t in range(wq.shape[1] // LANES):
            turned = norm_rotate(acc_q[:, pl.ds(t * LANES, LANES)], gain_q).astype(BF).astype(F32)
            turned = turned * HEAD_DIM ** (-0.5)
            qs[t, pl.ds(0, rows), :] = jnp.where(low_head, turned, 0.0).astype(BF)
            qs[t, pl.ds(rows, rows), :] = jnp.where(low_head, 0.0, turned).astype(BF)

    def gather_kv():
        width = wk.shape[1]
        for h in range(KV_HEADS):
            offset = (h % 2) * HEAD_DIM
            twice = jnp.where(square_r == offset + lax.rem(square_c, HEAD_DIM), 1.0, 0.0).astype(BF)
            base = (h // 2) * LANES
            for src, dst in ((base, k2), (width + base, v2)):
                both = kv[:, :, pl.ds(src, LANES)].reshape(seqs * rows, LANES)
                dst[h] = dot(both, twice).astype(BF)

    tiles = wq.shape[1] // LANES

    def attend(lo, hi):
        def body(t, carry):
            h = t // (tiles // KV_HEADS)
            scores = lax.dot_general(qs[t], k2[h], (((1,), (1,)), ((), ())), preferred_element_type=F32)
            top = jnp.max(scores, axis=-1, keepdims=True)
            weights = jnp.exp(scores - top)
            inverse = 1.0 / jnp.sum(weights, axis=-1, keepdims=True)
            mixed = dot((weights * inverse).astype(BF), v2[h])
            att[:, pl.ds(pl.multiple_of(t * LANES, LANES), LANES)] = jnp.where(
                low_head, mixed[:rows], mixed[rows:]).astype(BF)
            return carry
        lax.fori_loop(lo, hi, body, 0)

    def project(ref, owner):
        width = wo.shape[1]
        out[:, pl.ds(pl.multiple_of(owner * width, LANES), width)] = dot(att[...], ref).astype(BF)

    middle = max(1, (seqs - 1) // 3)
    step_x(0, 0)
    step_x(1, 0)
    step_x(0, 3)
    step_y(0, 1)
    step_z(0)
    step_x(1, 3)
    step_own(0)
    more(acc_k, fk, mate)
    step_own(1)
    more(acc_v, fv, mate)
    step_y(1, 1)
    step_z(1)
    step_x(2, 0)
    finish_kv()
    step_x(3, 0)
    step_own(2)
    more(acc_q, fq, mate)
    step_y(2, 1)
    step_z(2)
    for k in range(1, 1 + middle):
        relay(k)
    step_x(3, 3)
    step_y(3, 1)
    step_x(4, 0)
    step_z(3)
    step_y(2, 3)
    for k in range(1 + middle, 1 + 2 * middle):
        relay(k)
    step_x(5, 0)
    step_y(4, 1)
    finish_q()
    step_x(5, 2)
    step_z(4)
    for k in range(1 + 2 * middle, seqs):
        relay(k)
    step_x(4, 3)
    gather_kv()
    attend(tiles * 0 // 8, tiles * 2 // 8)
    step_y(5, 1)
    attend(tiles * 2 // 8, tiles * 4 // 8)
    step_y(5, 3)
    attend(tiles * 4 // 8, tiles * 8 // 8)
    project(wo[...], d)
    step_own(3)
    project(fo[mate], mate)
    for j in range(1, chips):
        project(fo[back(d, j)], back(d, j))
    for p in range(4, len(pieces)):
        step_c(p)
    for j in range(1, chips):
        project(fo[back(mate, j)], back(mate, j))
    for copy in sent:
        copy.wait_send()
    for there, copy in held_back:
        pl.when(there)(copy.wait_send)


def shards(n, groups, seqs, tokens, query_weight, key_weight, value_weight, out_weight, query_gain, key_gain):
    rows, width = tokens.shape[1], tokens.shape[2]
    local = tokens.reshape(rows, width)
    cuts = (1, 1, 2, 2)
    order = ((0, 0), (1, 0), (0, 3), (1, 3), (2, 0), (3, 0), (3, 3), (4, 0), (5, 0), (5, 2), (4, 3))
    count = sum(cuts)
    chips = n // 2
    kvw, qw = key_weight.shape[1], query_weight.shape[1]
    length = rows * seqs
    dma = pltpu.SemaphoreType.DMA
    vmem = pl.BlockSpec(memory_space=pltpu.VMEM)
    result = pl.pallas_call(
        functools.partial(kernel, n, groups, seqs, cuts, order),
        out_shape=jax.ShapeDtypeStruct((rows, width), BF),
        in_specs=[vmem] * 7,
        out_specs=vmem,
        scratch_shapes=[
            pltpu.VMEM((n,) + key_weight.shape, BF),
            pltpu.VMEM((n,) + value_weight.shape, BF),
            pltpu.VMEM((n,) + query_weight.shape, BF),
            pltpu.VMEM((n,) + out_weight.shape, BF),
            pltpu.VMEM((rows, LANES), F32),
            pltpu.VMEM((rows, LANES), F32),
            pltpu.VMEM((seqs, rows, 2 * kvw), BF),
            pltpu.VMEM((rows, kvw), F32),
            pltpu.VMEM((rows, kvw), F32),
            pltpu.VMEM((rows, qw), F32),
            pltpu.VMEM((qw // LANES, 2 * rows, LANES), BF),
            pltpu.VMEM((KV_HEADS, length, LANES), BF),
            pltpu.VMEM((KV_HEADS, length, LANES), BF),
            pltpu.VMEM((rows, qw), BF),
            dma((chips - 1, 4, count)), dma((chips - 1, 4, count)),
            dma((chips - 1, 2, count)), dma((chips - 1, 2, count)),
            dma((chips - 1, count)), dma((chips - 1, count)),
            dma((4,)), dma((4,)),
            dma((chips - 1, 4, count)), dma((chips - 1, 4, count)),
            dma((2, 2, seqs - 1)), dma((2, 2, seqs - 1)),
        ],
        compiler_params=pltpu.CompilerParams(
            collective_id=0, has_side_effects=True, vmem_limit_bytes=60 * 2 ** 20),
    )(local, key_weight, value_weight, query_weight, out_weight,
      query_gain.reshape(1, HEAD_DIM), key_gain.reshape(1, HEAD_DIM))
    return result.reshape(1, rows, width)


def solution(mesh):
    in_specs = (
        P(("grp", "dp"), "sp", None),
        P("dp", None),
        P("dp", None),
        P("dp", None),
        P(None, "dp"),
        P(),
        P(),
    )
    out_specs = P(("grp", "dp"), "sp", None)
    body = functools.partial(shards, mesh.shape["dp"], mesh.shape["grp"], mesh.shape["sp"])
    return jax.shard_map(body, mesh=mesh, in_specs=in_specs, out_specs=out_specs, check_vma=False)
```

time: 56.8 us -> 50.2 us (0.88)
  Pallas kernels: 50.6 us -> 48.1 us
  local copies, waits for them, and re-layouts: 4.14 us -> 1.98 us
  other arithmetic: 1.77 us -> 0 us
    pallas_call x1, Pallas kernels: 50.6 us -> 48.1 us  [shards(): pl.pallas_call(functools.partial(kernel, n, groups, seqs, cuts, order), o...]
    concatenate x2 -> x0, other arithmetic: 1.53 us -> none  [the longest x1 0.77 us: shards(): cos = jnp.concatenate([cosine] * 4, axis=1)]
    another operation x4 -> x0, local copies, waits for them, and re-layouts: 1.27 us -> none  [the longest x2 0.66 us: shards(): gk = jnp.tile(key_gain, 2).reshape(1, LANES)]
    unnamed x5 -> x1, local copies, waits for them, and re-layouts: 2.67 us -> 1.98 us
where the time goes in v2:
time: 50.2 us; the launch traced here: 50.1 us
  Pallas kernels  48.1 us (96%)
  local copies, waits for them, and re-layouts  1.98 us (4%)
    pallas_call x1, Pallas kernels, shards(): pl.pallas_call(functools.partial(kernel, n, groups, seqs, cuts, order), o...  48.1 us
    unnamed x1, local copies, waits for them, and re-layouts  1.98 us

profile of v2, /device:TPU:0, one launch (start us, length us, event | category | flops | bytes accessed | tf_op | source)
XLA Modules:
  0.0 50.1 jit_solution(339073201658631931)
XLA Ops:
  0.0 48.1 %shard_map.73 = bf16[160,2048]{1,0:T(8,128)(2,1)} custom-call(bf16[160,2048]{1,0:T(8,128)(2,1)} %bitcast.5, bf16[512,256]{1,0:T(8,128)(2,1)} %wk.1, bf16[512,256]{1,0:T(8,128)(2,1)} %wv.1, bf16[512,1024]{1,0:T(8,128)(2,1)} %wq.1, bf16[1024,512]{1,0:T(8,128)(2,1)} %wo.1, f32[1,64]{1,0:T(1,128)} %bitcast.6, f32[1,64]{1,0:T(1,128)} %bitcast.7), custom_call_target="tpu_custom_call" | custom-call | tf_op jit(solution)/shard_map/pallas_call | solution.py:343
  48.1 2.0 %copy.9 = bf16[1,160,2048]{2,1,0:T(8,128)(2,1)} copy(bf16[1,160,2048]{2,1,0:T(8,128)(2,1)} %bitcast.4) | data formatting | bytes 1310720

commit v3 on v2

--- a/solution.py
+++ b/solution.py
@@ -265,7 +265,7 @@
             att[:, pl.ds(pl.multiple_of(t * LANES, LANES), LANES)] = jnp.where(
                 low_head, mixed[:rows], mixed[rows:]).astype(BF)
             return carry
-        lax.fori_loop(lo, hi, body, 0)
+        lax.fori_loop(lo, hi, body, 0, unroll=True)
 
     def project(ref, owner):
         width = wo.shape[1]

time: 50.2 us -> 48.4 us (0.964)
  Pallas kernels: 48.1 us -> 46.2 us
    pallas_call x1, Pallas kernels: 48.1 us -> 46.2 us  [shards(): pl.pallas_call(functools.partial(kernel, n, groups, seqs, cuts, order), o...]
where the time goes in v3:
time: 48.4 us; the launch traced here: 48.2 us
  Pallas kernels  46.2 us (95%)
  local copies, waits for them, and re-layouts  1.98 us (4%)
    pallas_call x1, Pallas kernels, shards(): pl.pallas_call(functools.partial(kernel, n, groups, seqs, cuts, order), o...  46.2 us
    unnamed x1, local copies, waits for them, and re-layouts  1.98 us

profile of v3, /device:TPU:0, one launch (start us, length us, event | category | flops | bytes accessed | tf_op | source)
XLA Modules:
  0.0 48.2 jit_solution(17353948764420217796)
XLA Ops:
  0.0 46.2 %shard_map.73 = bf16[160,2048]{1,0:T(8,128)(2,1)} custom-call(bf16[160,2048]{1,0:T(8,128)(2,1)} %bitcast.5, bf16[512,256]{1,0:T(8,128)(2,1)} %wk.1, bf16[512,256]{1,0:T(8,128)(2,1)} %wv.1, bf16[512,1024]{1,0:T(8,128)(2,1)} %wq.1, bf16[1024,512]{1,0:T(8,128)(2,1)} %wo.1, f32[1,64]{1,0:T(1,128)} %bitcast.6, f32[1,64]{1,0:T(1,128)} %bitcast.7), custom_call_target="tpu_custom_call" | custom-call | tf_op jit(solution)/shard_map/pallas_call | solution.py:343
  46.2 2.0 %copy.9 = bf16[1,160,2048]{2,1,0:T(8,128)(2,1)} copy(bf16[1,160,2048]{2,1,0:T(8,128)(2,1)} %bitcast.4) | data formatting | bytes 1310720
